TPU v7x, 32 devices: a whole 2x2x4 slice. The times are simulated.
32 devices in a mesh: row: 8 (over z, y), col: 4 (over x, core).
Axes of the slice: x: 2, y: 2, z: 4, core: 2. Of those that a mesh axis runs over, the one named last changes fastest.
Arguments:
- tokens: bfloat16 [2, 32, 16, 2048], P(None, 'row', 'col'), may hold values from -6 to 6
- norm_gain: bfloat16 [2048], replicated, may hold values from 0.099609375 to 1.8984375
- w_mix_in: bfloat16 [2048, 1024], replicated, may hold values from -0.125 to 0.125
- w_mix_out: bfloat16 [1024, 2048], replicated, may hold values from -0.1875 to 0.1875
Outputs:
- mixed_tokens: bfloat16 [2, 16, 32, 2048], P(None, 'row', 'col')
All inputs are finite; a program needn't handle non-finite values.
Results may differ from a plain program's by a relative error of at most 0.013.
Values may be sent and summed in bfloat16 or wider, within the bound.
A program may use at most 64 MiB of HBM per device.

v0:
```python
import math

import jax
import jax.numpy as jnp
from jax import lax
from jax.sharding import PartitionSpec as P

G = 128


EPS = 1e-06
HIGHEST = lax.Precision.HIGHEST


def as_sent(x):

    def short(part):
        return part.astype(jnp.bfloat16) if part.dtype == jnp.float32 else part

    return jax.tree.map(short, x)


def phase_table(count_first, count_second, period, first_start):
    first_index = lax.iota(jnp.int32, count_first) + first_start
    second_index = lax.iota(jnp.int32, count_second)
    turn_count = first_index[:, None] * second_index[None, :] % period
    phases = turn_count.astype(jnp.float32) * (2.0 * math.pi / period)
    return (jnp.cos(phases), jnp.sin(phases))


def packed_table(group_width):
    source = lax.iota(jnp.int32, group_width)
    column = lax.iota(jnp.int32, group_width)
    pair_index = column // 2
    frequency = jnp.where(column == 1, group_width // 2, pair_index)
    use_sine = (column % 2 == 1) & (pair_index > 0)
    turn_count = source[:, None] * frequency[None, :] % group_width
    phases = turn_count.astype(jnp.float32) * (2.0 * math.pi / group_width)
    return jnp.where(use_sine[None, :], jnp.sin(phases), jnp.cos(phases)) / math.sqrt(group_width)


def body(tokens, norm_gain, w_mix_in, w_mix_out):
    seq_count, rows_here, cols_here, width = tokens.shape
    row_devices = lax.axis_size("row")
    col_devices = lax.axis_size("col")
    len_first = rows_here * row_devices
    len_second = cols_here * col_devices
    seq_length = len_first * len_second
    features = w_mix_in.shape[1]
    share = features // row_devices
    groups = features // G
    scaled = tokens.astype(jnp.float32)
    mean_square = jnp.mean(scaled * scaled, axis=-1, keepdims=True)
    normed = (scaled * lax.rsqrt(mean_square + EPS) * norm_gain.astype(jnp.float32)).astype(
        jnp.bfloat16
    )
    mixing_in = jnp.dot(
        normed.reshape(-1, width), w_mix_in, preferred_element_type=jnp.float32
    ).astype(jnp.bfloat16)
    grouped = mixing_in.astype(jnp.float32).reshape(seq_count, rows_here, cols_here, groups, G)
    first_cos, first_sin = phase_table(len_first, len_first, len_first, 0)
    first_cos = first_cos / math.sqrt(len_first)
    first_sin = first_sin / math.sqrt(len_first)
    col_start = lax.axis_index("col") * cols_here
    twist_cos, twist_sin = phase_table(cols_here, len_first, seq_length, col_start)
    twist_cos = twist_cos[None, :, None, :]
    twist_sin = twist_sin[None, :, None, :]
    packed = jnp.einsum("sabgc,cm->sabgm", grouped, packed_table(G), precision=HIGHEST)
    packed = packed.reshape(seq_count, rows_here, cols_here, features)
    turned = jnp.transpose(
        lax.all_to_all(
            packed.astype(jnp.bfloat16), "row", split_axis=3, concat_axis=1, tiled=True
        ).astype(packed.dtype),
        (0, 2, 3, 1),
    )
    real_out = jnp.einsum("njft,tk->njfk", turned, first_cos, precision=HIGHEST)
    imag_out = -jnp.einsum("njft,tk->njfk", turned, first_sin, precision=HIGHEST)
    spec_real = real_out * twist_cos + imag_out * twist_sin
    spec_imag = imag_out * twist_cos - real_out * twist_sin
    second_cos, second_sin = phase_table(len_second, len_second, len_second, 0)
    second_cos = second_cos / math.sqrt(len_second)
    second_sin = second_sin / math.sqrt(len_second)
    row_start = lax.axis_index("row") * share
    pair_global = row_start // 2 + lax.iota(jnp.int32, share // 2)
    head_pair = (pair_global % (G // 2) == 0)[:, None]
    real_in = lax.all_to_all(
        as_sent(spec_real), "col", split_axis=3, concat_axis=1, tiled=True
    ).astype(spec_real.dtype)
    imag_in = lax.all_to_all(
        as_sent(spec_imag), "col", split_axis=3, concat_axis=1, tiled=True
    ).astype(spec_imag.dtype)
    real_turned = jnp.transpose(real_in, (0, 3, 2, 1))
    imag_turned = jnp.transpose(imag_in, (0, 3, 2, 1))
    real_out = jnp.einsum("nqft,tk->nqfk", real_turned, second_cos, precision=HIGHEST) + jnp.einsum(
        "nqft,tk->nqfk", imag_turned, second_sin, precision=HIGHEST
    )
    imag_out = jnp.einsum("nqft,tk->nqfk", imag_turned, second_cos, precision=HIGHEST) - jnp.einsum(
        "nqft,tk->nqfk", real_turned, second_sin, precision=HIGHEST
    )
    out_shape = real_out.shape
    pair_shape = out_shape[:2] + (share // 2, 2, out_shape[3])
    real_pairs = real_out.reshape(pair_shape)
    imag_pairs = imag_out.reshape(pair_shape)
    even_real = real_pairs[:, :, :, 0, :]
    odd_real = real_pairs[:, :, :, 1, :]
    odd_imag = imag_pairs[:, :, :, 1, :]
    low_freq = jnp.where(head_pair, even_real, even_real + odd_imag)
    high_freq = jnp.where(head_pair, odd_real, even_real - odd_imag)
    joined = jnp.stack([low_freq, high_freq], axis=3).reshape(out_shape).astype(jnp.bfloat16)
    mixed = jnp.transpose(joined, (0, 3, 1, 2))
    piece = lax.all_to_all(mixed, "row", split_axis=1, concat_axis=3, tiled=True)
    paired = piece.reshape(piece.shape[:-1] + (groups, G // 2, 2))
    low_freq = paired[..., 0]
    high_freq = paired[..., 1]
    natural = jnp.concatenate(
        [low_freq, high_freq[..., :1], jnp.flip(high_freq[..., 1:], axis=-1)], axis=-1
    )
    project_piece = natural.reshape(piece.shape)
    flat = project_piece.reshape(-1, features)
    output = jnp.dot(flat, w_mix_out, preferred_element_type=jnp.float32).astype(jnp.bfloat16)
    return output.reshape(project_piece.shape[:-1] + (width,))


def solution(mesh):
    placed = (P(None, "row", "col", None), P(), P(), P())
    return jax.shard_map(
        body, mesh=mesh, in_specs=placed, out_specs=P(None, "row", "col", None), check_vma=False
    )
```

profile of v0, /device:TPU:0, one launch (start us, length us, event | category | flops | bytes accessed | tf_op | source)
XLA Modules:
  0.0 66.2 jit_solution(6027623879211877596)
XLA Ops:
  0.0 1.1 %fusion.3 = f32[2,4,4]{2,1,0:T(4,128)S(1)} fusion(bf16[2,4,4,2048]{3,2,1,0:T(4,128)(2,1)} %param.4), kind=kLoop, calls=%fused_computation.14 | loop fusion | flops 196576 | bytes 131200 | tf_op jit(solution)/shard_map/reduce_sum | solution.py:53
  1.1 0.7 %convert_element_type.63 = f32[2048]{0:T(1024)S(1)} convert(bf16[2048]{0:T(1024)(128)(2,1)} %param.5) | non-fusion elementwise | flops 2048 | bytes 12288 | tf_op jit(solution)/shard_map/convert_element_type | solution.py:54
  1.8 1.0 %fusion.5 = bf16[2,4,4,2048]{3,2,1,0:T(4,128)(2,1)S(1)} fusion(bf16[2,4,4,2048]{3,2,1,0:T(4,128)(2,1)} %param.4, f32[2048]{0:T(1024)S(1)} %convert_element_type.63, f32[2,4,4]{2,1,0:T(4,128)S(1)} %add_rsqrt_fusion), kind=kLoop, calls=%fused_computation.16 | loop fusion | flops 262144 | bytes 270464 | tf_op jit(solution)/shard_map/convert_element_type | solution.py:54
  2.9 3.0 %fusion = bf16[4,8,8,128]{3,1,2,0:T(8,128)(2,1)S(1)} fusion(bf16[32,2048]{1,0:T(8,128)(2,1)S(1)} %reshape.114, bf16[2048,1024]{1,0:T(8,128)(2,1)} %param.6), kind=kOutput, calls=%fused_computation.6 | convolution fusion | flops 134250496 | bytes 4390912 | tf_op jit(solution)/shard_map/dot_general | solution.py:57
  5.9 0.5 convolution_convert_fusion.2
  6.4 1.5 %copy.59 = bf16[2,4,4,8,128]{2,1,0,4,3:T(4,128)(2,1)S(1)} copy(bf16[2,4,4,8,128]{4,3,2,1,0:T(8,128)(2,1)S(1)} %convolution_convert_fusion.2) | data formatting | bytes 131072 | tf_op jit(solution)/shard_map/convert_element_type | solution.py:72
  7.9 4.6 %reshape.125 = bf16[8,2,2048]{2,1,0:T(2,128)(2,1)} reshape(bf16[1024,2,4,4]{3,2,1,0:T(4,128)(2,1)S(1)} %bitcast.84) | data formatting | bytes 131072
  12.5 7.3 %all-to-all-start = ((bf16[8,2,2048]{2,1,0:T(2,128)(2,1)}), bf16[8,2,2048]{2,1,0:T(2,128)(2,1)S(1)}, u32[]{:S(2)}, u32[]{:S(2)}) async-start(bf16[8,2,2048]{2,1,0:T(2,128)(2,1)} %reshape.125), calls=%async_computation | async-start | bytes 131072 | tf_op jit(solution)/shard_map/all_to_all | solution.py:71
  19.8 0.1 fusion.70
  20.0 6.8 %all-to-all-done = bf16[8,2,2048]{2,1,0:T(2,128)(2,1)S(1)} async-done(((bf16[8,2,2048]{2,1,0:T(2,128)(2,1)}), bf16[8,2,2048]{2,1,0:T(2,128)(2,1)S(1)}, u32[]{:S(2)}, u32[]{:S(2)}) %all-to-all-start) | async-done | bytes 65568 | tf_op jit(solution)/shard_map/all_to_all | solution.py:71
  26.7 4.5 %reshape.126 = bf16[1024,2,4,4]{3,2,1,0:T(4,128)(2,1)S(1)} reshape(bf16[8,2,2048]{2,1,0:T(2,128)(2,1)S(1)} %all-to-all-done) | data formatting | bytes 131072
  31.3 1.7 %copy.42 = bf16[2,4,4,8,128]{4,1,3,2,0:T(4,128)(2,1)S(1)} copy(bf16[2,4,4,8,128]{2,1,0,4,3:T(4,128)(2,1)S(1)} %bitcast.85) | data formatting | bytes 131072 | tf_op jit(solution)/shard_map/all_to_all | solution.py:71
  32.9 0.3 convolution_negate_fusion
  33.2 0.3 subtract_convert_fusion
  33.5 0.7 %copy.45 = bf16[2,4,128,32]{2,1,0,3:T(4,128)(2,1)} copy(bf16[2,4,128,32]{2,3,1,0:T(8,128)(2,1)S(1)} %get-tuple-element.9) | data formatting | bytes 131072 | tf_op jit(solution)/shard_map/convert_element_type | solution.py:18
  34.2 3.3 %all-to-all-start.2 = ((bf16[2,4,128,32]{2,1,0,3:T(4,128)(2,1)}), bf16[2,4,128,32]{2,1,0,3:T(4,128)(2,1)S(1)}, u32[]{:S(2)}, u32[]{:S(2)}) async-start(bf16[2,4,128,32]{2,1,0,3:T(4,128)(2,1)} %copy.45), calls=%async_computation.2 | async-start | bytes 131072 | tf_op jit(solution)/shard_map/all_to_all | solution.py:89
  37.5 0.7 copy.43
  38.1 3.4 %all-to-all-done.2 = bf16[2,4,128,32]{2,1,0,3:T(4,128)(2,1)S(1)} async-done(((bf16[2,4,128,32]{2,1,0,3:T(4,128)(2,1)}), bf16[2,4,128,32]{2,1,0,3:T(4,128)(2,1)S(1)}, u32[]{:S(2)}, u32[]{:S(2)}) %all-to-all-start.2) | async-done | bytes 65568 | tf_op jit(solution)/shard_map/all_to_all | solution.py:89
  41.6 3.3 %all-to-all-start.1 = ((bf16[2,4,128,32]{2,1,0,3:T(4,128)(2,1)}), bf16[2,4,128,32]{2,1,0,3:T(4,128)(2,1)S(1)}, u32[]{:S(2)}, u32[]{:S(2)}) async-start(bf16[2,4,128,32]{2,1,0,3:T(4,128)(2,1)} %copy.43), calls=%async_computation.1 | async-start | bytes 131072 | tf_op jit(solution)/shard_map/all_to_all | solution.py:86
  44.9 4.0 %all-to-all-done.1 = bf16[2,4,128,32]{2,1,0,3:T(4,128)(2,1)S(1)} async-done(((bf16[2,4,128,32]{2,1,0,3:T(4,128)(2,1)}), bf16[2,4,128,32]{2,1,0,3:T(4,128)(2,1)S(1)}, u32[]{:S(2)}, u32[]{:S(2)}) %all-to-all-start.1) | async-done | bytes 65568 | tf_op jit(solution)/shard_map/all_to_all | solution.py:86
  49.0 0.2 fusion.49
  49.2 0.2 fusion.47
  49.5 0.2 convolution_add_fusion
  49.7 0.2 convolution_subtract_fusion
  50.0 0.4 copy.48
  50.4 0.4 copy.47
  50.8 0.2 fusion.1
  51.0 0.1 pad_maximum_fusion
  51.1 0.3 copy.49
  51.5 9.3 %all_to_all.69 = bf16[2,16,8,128]{3,2,0,1:T(8,128)(2,1)S(1)} all-to-all(bf16[2,16,8,128]{3,2,0,1:T(8,128)(2,1)S(1)} %copy.49), channel_id=1, replica_groups=mesh['row'=8,'col'=4] {'row'}, dimensions={1} | all-to-all | bytes 131072 | tf_op jit(solution)/shard_map/all_to_all | solution.py:111
  60.7 0.6 copy.51
  61.3 0.2 fusion.108
  61.5 0.3 copy.52
  61.8 0.3 copy.53
  62.2 0.1 slice.34
  62.3 0.1 rev.4
  62.4 0.1 pad_maximum_fusion.1
  62.5 3.7 %convolution_convert_fusion = bf16[32,2048]{1,0:T(8,128)(2,1)} fusion(bf16[1024,2048]{1,0:T(8,128)(2,1)} %param.7, bf16[4,8,8,128]{3,2,1,0:T(8,128)(2,1)S(1)} %bitcast.96), kind=kOutput, calls=%fused_computation | convolution fusion | flops 134283264 | bytes 4390912 | tf_op jit(solution)/shard_map/dot_general | solution.py:120
  (9 shorter events, 0.1 us)
Async XLA Ops:
  12.5 14.2 %all-to-all-start = ((bf16[8,2,2048]{2,1,0:T(2,128)(2,1)}), bf16[8,2,2048]{2,1,0:T(2,128)(2,1)S(1)}, u32[]{:S(2)}, u32[]{:S(2)}) async-start(bf16[8,2,2048]{2,1,0:T(2,128)(2,1)} %reshape.125), calls=%async_computation | async-start | bytes 131072 | tf_op jit(solution)/shard_map/all_to_all | solution.py:71
  34.2 7.4 %all-to-all-start.2 = ((bf16[2,4,128,32]{2,1,0,3:T(4,128)(2,1)}), bf16[2,4,128,32]{2,1,0,3:T(4,128)(2,1)S(1)}, u32[]{:S(2)}, u32[]{:S(2)}) async-start(bf16[2,4,128,32]{2,1,0,3:T(4,128)(2,1)} %copy.45), calls=%async_computation.2 | async-start | bytes 131072 | tf_op jit(solution)/shard_map/all_to_all | solution.py:89
  41.6 7.4 %all-to-all-start.1 = ((bf16[2,4,128,32]{2,1,0,3:T(4,128)(2,1)}), bf16[2,4,128,32]{2,1,0,3:T(4,128)(2,1)S(1)}, u32[]{:S(2)}, u32[]{:S(2)}) async-start(bf16[2,4,128,32]{2,1,0,3:T(4,128)(2,1)} %copy.43), calls=%async_computation.1 | async-start | bytes 131072 | tf_op jit(solution)/shard_map/all_to_all | solution.py:86
where the time goes:
time: 66.7 us; the launch traced here: 66.2 us
  local copies, waits for them, and re-layouts  16.5 us (25%)
  waiting for transfers between devices  14.2 us (21%)
  starting transfers between devices  13.9 us (21%)
  blocking collectives  9.29 us (14%)
  matrix products  8.71 us (13%)
  other arithmetic  3.38 us (5%)
    all_to_all x1, blocking collectives, body(): lax.all_to_all(mixed, 'row', split_axis=1, concat_axis=3, tiled=True)  9.29 us
    unnamed x3, local copies, waits for them, and re-layouts  9.13 us
    all_to_all x1, starting transfers between devices, body(): lax.all_to_all(packed.astype(jnp.bfloat16), 'row', split_axis=3, concat_a...  7.31 us
    all_to_all x1, waiting for transfers between devices, body(): lax.all_to_all(packed.astype(jnp.bfloat16), 'row', split_axis=3, concat_a...  6.78 us
    all_to_all x1, waiting for transfers between devices, body(): lax.all_to_all(as_sent(spec_real), 'col', split_axis=3, concat_axis=1, ti...  4.04 us
    dot_general x1, matrix products, body(): jnp.dot(flat, w_mix_out, preferred_element_type=jnp.float32)  3.68 us
    all_to_all x1, waiting for transfers between devices, body(): lax.all_to_all(as_sent(spec_imag), 'col', split_axis=3, concat_axis=1, ti...  3.42 us
    all_to_all x1, starting transfers between devices, body(): lax.all_to_all(as_sent(spec_imag), 'col', split_axis=3, concat_axis=1, ti...  3.28 us
  transfers between devices with their start and end apart: 3, of which 3 were waited for; matrix products, arithmetic and copies ran while one was open for 1% of the time, Pallas kernels for 0%

commit v1 on v0

--- a/solution.py
+++ b/solution.py
@@ -1,9 +1,15 @@
+import functools
 import math
 
 import jax
 import jax.numpy as jnp
+import numpy as np
 from jax import lax
+from jax.experimental import pallas as pl
+from jax.experimental.pallas import tpu as pltpu
 from jax.sharding import PartitionSpec as P
+
+MESH = pl.DeviceIdType.MESH
 
 G = 128
 
@@ -39,7 +45,7 @@
     return jnp.where(use_sine[None, :], jnp.sin(phases), jnp.cos(phases)) / math.sqrt(group_width)
 
 
-def body(tokens, norm_gain, w_mix_in, w_mix_out):
+def staged_body(tokens, norm_gain, w_mix_in, w_mix_out):
     seq_count, rows_here, cols_here, width = tokens.shape
     row_devices = lax.axis_size("row")
     col_devices = lax.axis_size("col")
@@ -121,8 +127,247 @@
     return output.reshape(project_piece.shape[:-1] + (width,))
 
 
+class Plan:
+    def __init__(self, mesh, tokens_shape, features):
+        self.rows, self.cols = mesh.shape["row"], mesh.shape["col"]
+        self.devices = self.rows * self.cols
+        self.seqs, len_first, len_second, self.width = tokens_shape
+        self.len_first, self.len_second = len_first, len_second
+        self.features = features
+        self.groups = features // G
+        self.units = self.seqs * self.groups
+        self.t1, self.t2 = len_first // self.rows, len_second // self.cols
+        self.here = self.t1 * self.t2
+        self.length = len_first * len_second
+        self.q2, self.q1 = len_second // self.rows, len_first // self.cols
+
+    def fits(self):
+        if self.features % G or self.devices % self.units or self.length > 1024:
+            return False
+        if self.len_second % self.rows or self.len_first % self.cols:
+            return False
+        self.halves = self.devices // self.units
+        if self.rows % self.halves or self.here % 16 or self.q1 % 8:
+            return False
+        self.half_rows = self.rows // self.halves
+        return True
+
+    def tables(self):
+        row, col, a, b = np.meshgrid(
+            np.arange(self.rows), np.arange(self.cols), np.arange(self.t1), np.arange(self.t2), indexing="ij"
+        )
+        time = ((row * self.t1 + a) * self.len_second + col * self.t2 + b).reshape(-1)
+        row, col, a, b = np.meshgrid(
+            np.arange(self.rows), np.arange(self.cols), np.arange(self.q2), np.arange(self.q1), indexing="ij"
+        )
+        freq = (col * self.q1 + b + self.len_first * (row * self.q2 + a)).reshape(self.halves, -1)
+        turn = 2.0 * np.pi / self.length * (freq[:, :, None] * time[None, None, :] % self.length)
+        scale = 1.0 / math.sqrt(self.length * G)
+        first = 2.0 ** round(math.log2(scale) / 2)
+        position = np.concatenate([np.cos(turn), np.sin(turn)], axis=1) * first
+        channel = np.arange(G)
+        turn = 2.0 * np.pi / G * (channel[:, None] * channel[None, :] % G)
+        channel = np.concatenate([np.cos(turn), -np.sin(turn)], axis=0) * (scale / first)
+        return jnp.asarray(position, jnp.bfloat16), jnp.asarray(channel, jnp.bfloat16)
+
+
+VMEM_BYTES = 67043328
+IN_CHUNKS = 4
+OUT_CHUNKS = 4
+
+
+def mix_kernel(
+    plan, tokens_hbm, gain_hbm, w_in_hbm, w_out_hbm, table_hbm, channel_hbm, out_ref,
+    tokens_v, gain_v, w_in_v, w_out_v, table_v, channel_v, flat_v,
+    x_send, x_recv, s_send, s_recv,
+    load_sem, in_sem, out_sem, x_send_sem, x_recv_sem, s_send_sem, s_recv_sem,
+):
+    row, col = lax.axis_index("row"), lax.axis_index("col")
+    me = row * plan.cols + col
+    half = row // plan.half_rows
+    unit = lax.rem(me, plan.units)
+    place = lambda d: {"row": d // plan.cols, "col": lax.rem(d, plan.cols)}
+
+    barrier = pltpu.get_barrier_semaphore()
+
+    def greet(i, carry):
+        pl.semaphore_signal(
+            barrier, inc=1, device_id=place(lax.rem(me + i, plan.devices)), device_id_type=MESH
+        )
+        return carry
+
+    token_load = pltpu.make_async_copy(tokens_hbm, tokens_v, load_sem.at[0])
+    gain_load = pltpu.make_async_copy(gain_hbm, gain_v, load_sem.at[1])
+    table_load = pltpu.make_async_copy(table_hbm.at[half], table_v, load_sem.at[2])
+    channel_load = pltpu.make_async_copy(channel_hbm, channel_v, load_sem.at[3])
+    depth = plan.width // IN_CHUNKS
+    in_loads = [
+        pltpu.make_async_copy(
+            w_in_hbm.at[pl.ds(j * depth, depth)], w_in_v.at[pl.ds(j * depth, depth)], in_sem.at[j]
+        )
+        for j in range(IN_CHUNKS)
+    ]
+    span = plan.width // OUT_CHUNKS
+    out_load = pltpu.make_async_copy(w_out_hbm, w_out_v, out_sem.at[0])
+    token_load.start()
+    gain_load.start()
+    for load in in_loads:
+        load.start()
+    table_load.start()
+    channel_load.start()
+    out_load.start()
+    lax.fori_loop(1, plan.devices, greet, 0)
+
+    token_load.wait()
+    for s in range(plan.seqs):
+        for a in range(plan.t1):
+            flat_v[pl.ds((s * plan.t1 + a) * plan.t2, plan.t2), :] = tokens_v[s, a].astype(jnp.float32)
+    scaled = flat_v[...]
+    mean_square = jnp.mean(scaled * scaled, axis=-1, keepdims=True)
+    gain_load.wait()
+    gain = gain_v[...].astype(jnp.float32).reshape(1, plan.width)
+    normed = (scaled * lax.rsqrt(mean_square + EPS) * gain).astype(jnp.bfloat16)
+    mixing = None
+    for j in range(IN_CHUNKS):
+        in_loads[j].wait()
+        part = jnp.dot(
+            normed[:, j * depth : (j + 1) * depth],
+            w_in_v[pl.ds(j * depth, depth), :],
+            preferred_element_type=jnp.float32,
+        )
+        mixing = part if mixing is None else mixing + part
+    mixing = mixing.astype(jnp.bfloat16)
+    for g in range(plan.groups):
+        for s in range(plan.seqs):
+            x_send[g * plan.seqs + s] = mixing[s * plan.here : (s + 1) * plan.here, g * G : (g + 1) * G]
+
+    pl.semaphore_wait(barrier, plan.devices - 1)
+
+    def x_copy(source, target):
+        return pltpu.make_async_remote_copy(
+            src_ref=x_send.at[lax.rem(target, plan.units)],
+            dst_ref=x_recv.at[source],
+            send_sem=x_send_sem.at[target],
+            recv_sem=x_recv_sem.at[source],
+            device_id=place(target),
+            device_id_type=MESH,
+        )
+
+    def x_start(i, carry):
+        x_copy(me, lax.rem(me + i, plan.devices)).start()
+        return carry
+
+    lax.fori_loop(1, plan.devices, x_start, 0)
+    x_recv[me] = x_send[unit]
+    table_load.wait()
+    channel_load.wait()
+
+    def x_wait(i, carry):
+        x_copy(lax.rem(me + i, plan.devices), me).wait_recv()
+        return carry
+
+    lax.fori_loop(1, plan.devices, x_wait, 0)
+    values = x_recv[...].reshape(plan.length, G)
+    turned = jnp.dot(table_v[...], values, preferred_element_type=jnp.float32).astype(jnp.bfloat16)
+    owned = plan.length // plan.halves
+    both = jnp.concatenate([turned[:owned], turned[owned:]], axis=1)
+    spectrum = jnp.dot(both, channel_v[...], preferred_element_type=jnp.float32).astype(jnp.bfloat16)
+    s_send[...] = spectrum.reshape(s_send.shape)
+
+    def s_copy(source, target):
+        return pltpu.make_async_remote_copy(
+            src_ref=s_send.at[target],
+            dst_ref=s_recv.at[source],
+            send_sem=s_send_sem.at[target],
+            recv_sem=s_recv_sem.at[source],
+            device_id=place(half * plan.units + target),
+            device_id_type=MESH,
+        )
+
+    def s_start(i, carry):
+        s_copy(unit, lax.rem(unit + i, plan.units)).start()
+        return carry
+
+    lax.fori_loop(1, plan.units, s_start, 0)
+    s_recv[unit] = s_send[unit]
+    out_load.wait()
+
+    def s_wait(i, carry):
+        s_copy(lax.rem(unit + i, plan.units), unit).wait_recv()
+        return carry
+
+    lax.fori_loop(1, plan.units, s_wait, 0)
+    mixed = jnp.concatenate(
+        [
+            jnp.concatenate([s_recv[g * plan.seqs + s] for s in range(plan.seqs)], axis=0)
+            for g in range(plan.groups)
+        ],
+        axis=1,
+    )
+    for j in range(OUT_CHUNKS):
+        piece = jnp.dot(
+            mixed, w_out_v[:, pl.ds(j * span, span)], preferred_element_type=jnp.float32
+        )
+        for s in range(plan.seqs):
+            for q in range(plan.q2):
+                start = (s * plan.q2 + q) * plan.q1
+                out_ref[s, q, :, pl.ds(j * span, span)] = piece[start : start + plan.q1].astype(jnp.bfloat16)
+
+    def x_sent(i, carry):
+        x_copy(me, lax.rem(me + i, plan.devices)).wait_send()
+        return carry
+
+    def s_sent(i, carry):
+        s_copy(unit, lax.rem(unit + i, plan.units)).wait_send()
+        return carry
+
+    lax.fori_loop(1, plan.devices, x_sent, 0)
+    lax.fori_loop(1, plan.units, s_sent, 0)
+
+
+def kernel_body(plan, tokens, norm_gain, w_mix_in, w_mix_out):
+    table, channel = plan.tables()
+    bf16 = jnp.bfloat16
+    dma = pltpu.SemaphoreType.DMA
+    return pl.pallas_call(
+        functools.partial(mix_kernel, plan),
+        out_shape=jax.ShapeDtypeStruct((plan.seqs, plan.q2, plan.q1, plan.width), bf16),
+        in_specs=[pl.BlockSpec(memory_space=pl.ANY)] * 6,
+        out_specs=pl.BlockSpec(memory_space=pltpu.VMEM),
+        scratch_shapes=[
+            pltpu.VMEM(tokens.shape, bf16),
+            pltpu.VMEM(norm_gain.shape, bf16),
+            pltpu.VMEM(w_mix_in.shape, bf16),
+            pltpu.VMEM(w_mix_out.shape, bf16),
+            pltpu.VMEM(table.shape[1:], bf16),
+            pltpu.VMEM(channel.shape, bf16),
+            pltpu.VMEM((plan.seqs * plan.here, plan.width), jnp.float32),
+            pltpu.VMEM((plan.units, plan.here, G), bf16),
+            pltpu.VMEM((plan.devices, plan.here, G), bf16),
+            pltpu.VMEM((plan.units, plan.q2 * plan.q1, G), bf16),
+            pltpu.VMEM((plan.units, plan.q2 * plan.q1, G), bf16),
+            dma((4,)),
+            dma((IN_CHUNKS,)),
+            dma((OUT_CHUNKS,)),
+            dma((plan.devices,)),
+            dma((plan.devices,)),
+            dma((plan.units,)),
+            dma((plan.units,)),
+        ],
+        compiler_params=pltpu.CompilerParams(
+            collective_id=0, has_side_effects=True, vmem_limit_bytes=VMEM_BYTES
+        ),
+    )(tokens, norm_gain, w_mix_in, w_mix_out, table, channel)
+
+
 def solution(mesh):
     placed = (P(None, "row", "col", None), P(), P(), P())
-    return jax.shard_map(
-        body, mesh=mesh, in_specs=placed, out_specs=P(None, "row", "col", None), check_vma=False
-    )
+
+    def run(tokens, norm_gain, w_mix_in, w_mix_out):
+        plan = Plan(mesh, tokens.shape, w_mix_in.shape[1])
+        body = functools.partial(kernel_body, plan) if plan.fits() else staged_body
+        return jax.shard_map(
+            body, mesh=mesh, in_specs=placed, out_specs=P(None, "row", "col", None), check_vma=False
+        )(tokens, norm_gain, w_mix_in, w_mix_out)
+
+    return run

time: 66.7 us -> 20.9 us (0.31)
  Pallas kernels: 0 us -> 19.1 us
  local copies, waits for them, and re-layouts: 16.5 us -> 1.57 us
  waiting for transfers between devices: 14.2 us -> 0 us
  starting transfers between devices: 13.9 us -> 0 us
  blocking collectives: 9.29 us -> 0 us
  matrix products: 8.71 us -> 0 us
  other arithmetic: 3.38 us -> 0 us
    pallas_call x0 -> x1, Pallas kernels: none -> 19.1 us  [kernel_body(): pl.pallas_call(functools.partial(mix_kernel, plan), out_shape=jax.ShapeDt...]
    all_to_all x3 -> x0, waiting for transfers between devices: 14.2 us -> none  [the longest x1 6.78 us: body(): lax.all_to_all(packed.astype(jnp.bfloat16), 'row', split_axis=3, concat_a...]
    all_to_all x3 -> x0, starting transfers between devices: 13.9 us -> none  [the longest x1 7.31 us: body(): lax.all_to_all(packed.astype(jnp.bfloat16), 'row', split_axis=3, concat_a...]
    all_to_all x1 -> x0, blocking collectives: 9.29 us -> none  [body(): lax.all_to_all(mixed, 'row', split_axis=1, concat_axis=3, tiled=True)]
    dot_general x9 -> x0, matrix products: 8.71 us -> none  [the longest x1 3.68 us: body(): jnp.dot(flat, w_mix_out, preferred_element_type=jnp.float32)]
    unnamed x3 -> x1, local copies, waits for them, and re-layouts: 9.13 us -> 1.57 us
    convert_element_type x3 -> x0, local copies, waits for them, and re-layouts: 2.84 us -> none  [the longest x1 1.52 us: body(): packed.astype(jnp.bfloat16)]
    all_to_all x4 -> x0, local copies, waits for them, and re-layouts: 2.29 us -> none  [the longest x1 1.69 us: body(): lax.all_to_all(packed.astype(jnp.bfloat16), 'row', split_axis=3, concat_a...]
  transfers between devices with their start and end apart: 3 -> 0, of which waited for: 3 -> 0; matrix products, arithmetic and copies ran while one was open for 1% -> 0% of each run, Pallas kernels for 0% -> 0%
where the time goes in v1:
time: 20.9 us; the launch traced here: 20.7 us
  Pallas kernels  19.1 us (91%)
  local copies, waits for them, and re-layouts  1.57 us (8%)
    pallas_call x1, Pallas kernels, kernel_body(): pl.pallas_call(functools.partial(mix_kernel, plan), out_shape=jax.ShapeDt...  19.1 us
    unnamed x1, local copies, waits for them, and re-layouts  1.57 us

profile of v1, /device:TPU:0, one launch (start us, length us, event | category | flops | bytes accessed | tf_op | source)
XLA Modules:
  0.0 20.7 jit_solution(6045312716086674348)
XLA Ops:
  0.0 19.1 %shard_map.64 = bf16[2,2,8,2048]{3,2,1,0:T(8,128)(2,1)} custom-call(bf16[2,4,4,2048]{3,2,1,0:T(4,128)(2,1)} %tokens_hbm.1, bf16[2048]{0:T(1024)(128)(2,1)} %gain_hbm.1, bf16[2048,1024]{1,0:T(8,128)(2,1)} %w_in_hbm.1, bf16[1024,2048]{1,0:T(8,128)(2,1)} %w_out_hbm.1, bf16[2,512,512]{2,1,0:T(8,128)(2,1)} %constant.4.clone.table_hbm, ...), custom_call_target="tpu_custom_call" | custom-call | tf_op jit(solution)/shard_map/pallas_call | solution.py:332
  19.2 1.6 %copy.8 = bf16[2,2,8,2048]{3,2,1,0:T(8,128)(2,1)} copy(bf16[2,2,8,2048]{3,2,1,0:T(8,128)(2,1)} %shard_map.64) | data formatting | bytes 262144

commit v2 on v1

--- a/solution.py
+++ b/solution.py
@@ -144,6 +144,8 @@
     def fits(self):
         if self.features % G or self.devices % self.units or self.length > 1024:
             return False
+        if self.devices & (self.devices - 1) or self.units & (self.units - 1):
+            return False
         if self.len_second % self.rows or self.len_first % self.cols:
             return False
         self.halves = self.devices // self.units
@@ -171,7 +173,7 @@
         return jnp.asarray(position, jnp.bfloat16), jnp.asarray(channel, jnp.bfloat16)
 
 
-VMEM_BYTES = 67043328
+VMEM_BYTES = 16 * 1024 * 1024
 IN_CHUNKS = 4
 OUT_CHUNKS = 4
 
@@ -190,11 +192,14 @@
 
     barrier = pltpu.get_barrier_semaphore()
 
-    def greet(i, carry):
-        pl.semaphore_signal(
-            barrier, inc=1, device_id=place(lax.rem(me + i, plan.devices)), device_id_type=MESH
-        )
-        return carry
+    flips = []
+    bit = 1
+    while bit < plan.devices:
+        flips.append((bit, bit * (1 - 2 * lax.rem(me // bit, 2))))
+        bit *= 2
+
+    def partner(mask):
+        return me + sum(step for bit, step in flips if mask & bit)
 
     token_load = pltpu.make_async_copy(tokens_hbm, tokens_v, load_sem.at[0])
     gain_load = pltpu.make_async_copy(gain_hbm, gain_v, load_sem.at[1])
@@ -216,7 +221,8 @@
     table_load.start()
     channel_load.start()
     out_load.start()
-    lax.fori_loop(1, plan.devices, greet, 0)
+    for mask in range(plan.devices - 1, 0, -1):
+        pl.semaphore_signal(barrier, inc=1, device_id=place(partner(mask)), device_id_type=MESH)
 
     token_load.wait()
     for s in range(plan.seqs):
@@ -253,11 +259,8 @@
             device_id_type=MESH,
         )
 
-    def x_start(i, carry):
-        x_copy(me, lax.rem(me + i, plan.devices)).start()
-        return carry
-
-    lax.fori_loop(1, plan.devices, x_start, 0)
+    for mask in range(plan.devices - 1, 0, -1):
+        x_copy(me, partner(mask)).start()
     x_recv[me] = x_send[unit]
     table_load.wait()
     channel_load.wait()
@@ -284,11 +287,8 @@
             device_id_type=MESH,
         )
 
-    def s_start(i, carry):
-        s_copy(unit, lax.rem(unit + i, plan.units)).start()
-        return carry
-
-    lax.fori_loop(1, plan.units, s_start, 0)
+    for mask in range(plan.units - 1, 0, -1):
+        s_copy(unit, lax.rem(partner(mask), plan.units)).start()
     s_recv[unit] = s_send[unit]
     out_load.wait()
 
@@ -332,7 +332,7 @@
     return pl.pallas_call(
         functools.partial(mix_kernel, plan),
         out_shape=jax.ShapeDtypeStruct((plan.seqs, plan.q2, plan.q1, plan.width), bf16),
-        in_specs=[pl.BlockSpec(memory_space=pl.ANY)] * 6,
+        in_specs=[pl.BlockSpec(memory_space=pltpu.HBM)] * 6,
         out_specs=pl.BlockSpec(memory_space=pltpu.VMEM),
         scratch_shapes=[
             pltpu.VMEM(tokens.shape, bf16),
@@ -357,7 +357,10 @@
         compiler_params=pltpu.CompilerParams(
             collective_id=0, has_side_effects=True, vmem_limit_bytes=VMEM_BYTES
         ),
-    )(tokens, norm_gain, w_mix_in, w_mix_out, table, channel)
+    )(*[
+        pltpu.with_memory_space_constraint(x, pltpu.HBM)
+        for x in (tokens, norm_gain, w_mix_in, w_mix_out, table, channel)
+    ])
 
 
 def solution(mesh):

time: 20.9 us -> 19.1 us (0.914)
  local copies, waits for them, and re-layouts: 1.57 us -> 0.66 us
  Pallas kernels: 19.1 us -> 18.3 us
    unnamed x1, local copies, waits for them, and re-layouts: 1.57 us -> 0.66 us
    pallas_call x1, Pallas kernels: 19.1 us -> 18.3 us  [kernel_body(): pl.pallas_call(functools.partial(mix_kernel, plan), out_shape=jax.ShapeDt...]
where the time goes in v2:
time: 19.1 us; the launch traced here: 19 us
  Pallas kernels  18.3 us (96%)
  local copies, waits for them, and re-layouts  0.66 us (3%)
    pallas_call x1, Pallas kernels, kernel_body(): pl.pallas_call(functools.partial(mix_kernel, plan), out_shape=jax.ShapeDt...  18.3 us
    unnamed x1, local copies, waits for them, and re-layouts  0.66 us

profile of v2, /device:TPU:0, one launch (start us, length us, event | category | flops | bytes accessed | tf_op | source)
XLA Modules:
  0.0 19.0 jit_solution(14734927415890481860)
XLA Ops:
  0.0 18.3 %shard_map.64 = bf16[2,2,8,2048]{3,2,1,0:T(8,128)(2,1)S(1)} custom-call(bf16[2,4,4,2048]{3,2,1,0:T(4,128)(2,1)} %tokens_hbm.1, bf16[2048]{0:T(1024)(128)(2,1)} %gain_hbm.1, bf16[2048,1024]{1,0:T(8,128)(2,1)} %w_in_hbm.1, bf16[1024,2048]{1,0:T(8,128)(2,1)} %w_out_hbm.1, bf16[2,512,512]{2,1,0:T(8,128)(2,1)} %constant.4.clone.table_hbm, ...), custom_call_target="tpu_custom_call" | custom-call | tf_op jit(solution)/shard_map/pallas_call | solution.py:332
  18.3 0.7 %copy.8 = bf16[2,2,8,2048]{3,2,1,0:T(8,128)(2,1)} copy(bf16[2,2,8,2048]{3,2,1,0:T(8,128)(2,1)S(1)} %shard_map.64) | data formatting | bytes 262144

commit v3 on v2

--- a/solution.py
+++ b/solution.py
@@ -135,38 +135,38 @@
         self.len_first, self.len_second = len_first, len_second
         self.features = features
         self.groups = features // G
-        self.units = self.seqs * self.groups
         self.t1, self.t2 = len_first // self.rows, len_second // self.cols
         self.here = self.t1 * self.t2
         self.length = len_first * len_second
         self.q2, self.q1 = len_second // self.rows, len_first // self.cols
 
     def fits(self):
-        if self.features % G or self.devices % self.units or self.length > 1024:
+        if self.features % G or self.devices != 4 * self.groups or self.length > 1024:
             return False
-        if self.devices & (self.devices - 1) or self.units & (self.units - 1):
+        if self.devices & (self.devices - 1) or self.rows % 2 or self.cols % 2:
             return False
         if self.len_second % self.rows or self.len_first % self.cols:
             return False
-        self.halves = self.devices // self.units
-        if self.rows % self.halves or self.here % 16 or self.q1 % 8:
+        if self.here % 16 or self.q1 % 8 or self.q2 * self.q1 % 16:
             return False
-        self.half_rows = self.rows // self.halves
+        self.half_rows, self.side_cols = self.rows // 2, self.cols // 2
+        self.span = self.devices // 2
         return True
 
     def tables(self):
         row, col, a, b = np.meshgrid(
             np.arange(self.rows), np.arange(self.cols), np.arange(self.t1), np.arange(self.t2), indexing="ij"
         )
-        time = ((row * self.t1 + a) * self.len_second + col * self.t2 + b).reshape(-1)
+        time = (row * self.t1 + a) * self.len_second + col * self.t2 + b
+        time = np.stack([part.reshape(-1) for part in np.split(time, 2, axis=1)])
         row, col, a, b = np.meshgrid(
             np.arange(self.rows), np.arange(self.cols), np.arange(self.q2), np.arange(self.q1), indexing="ij"
         )
-        freq = (col * self.q1 + b + self.len_first * (row * self.q2 + a)).reshape(self.halves, -1)
-        turn = 2.0 * np.pi / self.length * (freq[:, :, None] * time[None, None, :] % self.length)
+        freq = (col * self.q1 + b + self.len_first * (row * self.q2 + a)).reshape(2, -1)
+        turn = 2.0 * np.pi / self.length * (freq[:, None, :, None] * time[None, :, None, :] % self.length)
         scale = 1.0 / math.sqrt(self.length * G)
         first = 2.0 ** round(math.log2(scale) / 2)
-        position = np.concatenate([np.cos(turn), np.sin(turn)], axis=1) * first
+        position = np.concatenate([np.cos(turn), np.sin(turn)], axis=2) * first
         channel = np.arange(G)
         turn = 2.0 * np.pi / G * (channel[:, None] * channel[None, :] % G)
         channel = np.concatenate([np.cos(turn), -np.sin(turn)], axis=0) * (scale / first)
@@ -186,8 +186,12 @@
 ):
     row, col = lax.axis_index("row"), lax.axis_index("col")
     me = row * plan.cols + col
-    half = row // plan.half_rows
-    unit = lax.rem(me, plan.units)
+    half, side = row // plan.half_rows, col // plan.side_cols
+    in_half = lax.rem(me, plan.span)
+    group_of = lambda d: lax.rem(d // plan.cols, plan.half_rows) * plan.side_cols + lax.rem(d, plan.side_cols)
+    in_side = lambda d: d // plan.cols * plan.side_cols + lax.rem(d, plan.side_cols)
+    x_masks = [m for m in range(plan.devices - 1, 0, -1) if not m & plan.side_cols]
+    s_masks = list(range(plan.span - 1, 0, -1))
     place = lambda d: {"row": d // plan.cols, "col": lax.rem(d, plan.cols)}
 
     barrier = pltpu.get_barrier_semaphore()
@@ -203,7 +207,7 @@
 
     token_load = pltpu.make_async_copy(tokens_hbm, tokens_v, load_sem.at[0])
     gain_load = pltpu.make_async_copy(gain_hbm, gain_v, load_sem.at[1])
-    table_load = pltpu.make_async_copy(table_hbm.at[half], table_v, load_sem.at[2])
+    table_load = pltpu.make_async_copy(table_hbm.at[half, side], table_v, load_sem.at[2])
     channel_load = pltpu.make_async_copy(channel_hbm, channel_v, load_sem.at[3])
     depth = plan.width // IN_CHUNKS
     in_loads = [
@@ -218,10 +222,8 @@
     gain_load.start()
     for load in in_loads:
         load.start()
-    table_load.start()
-    channel_load.start()
-    out_load.start()
-    for mask in range(plan.devices - 1, 0, -1):
+    peers = [m for m in range(plan.devices - 1, 0, -1) if m in x_masks or m in s_masks]
+    for mask in peers:
         pl.semaphore_signal(barrier, inc=1, device_id=place(partner(mask)), device_id_type=MESH)
 
     token_load.wait()
@@ -244,38 +246,45 @@
         mixing = part if mixing is None else mixing + part
     mixing = mixing.astype(jnp.bfloat16)
     for g in range(plan.groups):
-        for s in range(plan.seqs):
-            x_send[g * plan.seqs + s] = mixing[s * plan.here : (s + 1) * plan.here, g * G : (g + 1) * G]
-
-    pl.semaphore_wait(barrier, plan.devices - 1)
+        x_send[g] = mixing[:, g * G : (g + 1) * G]
+    table_load.start()
+    channel_load.start()
+    out_load.start()
+
+    pl.semaphore_wait(barrier, len(peers))
 
     def x_copy(source, target):
         return pltpu.make_async_remote_copy(
-            src_ref=x_send.at[lax.rem(target, plan.units)],
-            dst_ref=x_recv.at[source],
-            send_sem=x_send_sem.at[target],
-            recv_sem=x_recv_sem.at[source],
+            src_ref=x_send.at[group_of(target)],
+            dst_ref=x_recv.at[in_side(source)],
+            send_sem=x_send_sem.at[in_side(target)],
+            recv_sem=x_recv_sem.at[in_side(source)],
             device_id=place(target),
             device_id_type=MESH,
         )
 
-    for mask in range(plan.devices - 1, 0, -1):
+    for mask in x_masks:
         x_copy(me, partner(mask)).start()
-    x_recv[me] = x_send[unit]
+    x_recv[in_side(me)] = x_send[group_of(me)]
     table_load.wait()
     channel_load.wait()
-
-    def x_wait(i, carry):
-        x_copy(lax.rem(me + i, plan.devices), me).wait_recv()
-        return carry
-
-    lax.fori_loop(1, plan.devices, x_wait, 0)
-    values = x_recv[...].reshape(plan.length, G)
+    for mask in reversed(x_masks):
+        x_copy(partner(mask), me).wait_recv()
+    values = jnp.concatenate(
+        [
+            x_recv[:, pl.ds(s * plan.here, plan.here), :].reshape(plan.span * plan.here, G)
+            for s in range(plan.seqs)
+        ],
+        axis=1,
+    )
     turned = jnp.dot(table_v[...], values, preferred_element_type=jnp.float32).astype(jnp.bfloat16)
-    owned = plan.length // plan.halves
-    both = jnp.concatenate([turned[:owned], turned[owned:]], axis=1)
-    spectrum = jnp.dot(both, channel_v[...], preferred_element_type=jnp.float32).astype(jnp.bfloat16)
-    s_send[...] = spectrum.reshape(s_send.shape)
+    owned = plan.length // 2
+    piece = plan.q2 * plan.q1
+    for s in range(plan.seqs):
+        lanes = slice(s * G, (s + 1) * G)
+        both = jnp.concatenate([turned[:owned, lanes], turned[owned:, lanes]], axis=1)
+        spectrum = jnp.dot(both, channel_v[...], preferred_element_type=jnp.float32)
+        s_send[:, pl.ds(s * piece, piece), :] = spectrum.astype(jnp.bfloat16).reshape(plan.span, piece, G)
 
     def s_copy(source, target):
         return pltpu.make_async_remote_copy(
@@ -283,27 +292,23 @@
             dst_ref=s_recv.at[source],
             send_sem=s_send_sem.at[target],
             recv_sem=s_recv_sem.at[source],
-            device_id=place(half * plan.units + target),
+            device_id=place(half * plan.span + target),
             device_id_type=MESH,
         )
 
-    for mask in range(plan.units - 1, 0, -1):
-        s_copy(unit, lax.rem(partner(mask), plan.units)).start()
-    s_recv[unit] = s_send[unit]
+    for mask in s_masks:
+        s_copy(in_half, lax.rem(partner(mask), plan.span)).start()
+    s_recv[in_half] = s_send[in_half]
     out_load.wait()
-
-    def s_wait(i, carry):
-        s_copy(lax.rem(unit + i, plan.units), unit).wait_recv()
-        return carry
-
-    lax.fori_loop(1, plan.units, s_wait, 0)
-    mixed = jnp.concatenate(
-        [
-            jnp.concatenate([s_recv[g * plan.seqs + s] for s in range(plan.seqs)], axis=0)
-            for g in range(plan.groups)
-        ],
-        axis=1,
-    )
+    for mask in reversed(s_masks):
+        s_copy(lax.rem(partner(mask), plan.span), in_half).wait_recv()
+
+    def sides_sum(g):
+        first = g // plan.side_cols * plan.cols + g % plan.side_cols
+        total = s_recv[first].astype(jnp.float32) + s_recv[first + plan.side_cols].astype(jnp.float32)
+        return total.astype(jnp.bfloat16)
+
+    mixed = jnp.concatenate([sides_sum(g) for g in range(plan.groups)], axis=1)
     for j in range(OUT_CHUNKS):
         piece = jnp.dot(
             mixed, w_out_v[:, pl.ds(j * span, span)], preferred_element_type=jnp.float32
@@ -313,16 +318,10 @@
                 start = (s * plan.q2 + q) * plan.q1
                 out_ref[s, q, :, pl.ds(j * span, span)] = piece[start : start + plan.q1].astype(jnp.bfloat16)
 
-    def x_sent(i, carry):
-        x_copy(me, lax.rem(me + i, plan.devices)).wait_send()
-        return carry
-
-    def s_sent(i, carry):
-        s_copy(unit, lax.rem(unit + i, plan.units)).wait_send()
-        return carry
-
-    lax.fori_loop(1, plan.devices, x_sent, 0)
-    lax.fori_loop(1, plan.units, s_sent, 0)
+    for mask in x_masks:
+        x_copy(me, partner(mask)).wait_send()
+    for mask in s_masks:
+        s_copy(in_half, lax.rem(partner(mask), plan.span)).wait_send()
 
 
 def kernel_body(plan, tokens, norm_gain, w_mix_in, w_mix_out):
@@ -339,20 +338,20 @@
             pltpu.VMEM(norm_gain.shape, bf16),
             pltpu.VMEM(w_mix_in.shape, bf16),
             pltpu.VMEM(w_mix_out.shape, bf16),
-            pltpu.VMEM(table.shape[1:], bf16),
+            pltpu.VMEM(table.shape[2:], bf16),
             pltpu.VMEM(channel.shape, bf16),
             pltpu.VMEM((plan.seqs * plan.here, plan.width), jnp.float32),
-            pltpu.VMEM((plan.units, plan.here, G), bf16),
-            pltpu.VMEM((plan.devices, plan.here, G), bf16),
-            pltpu.VMEM((plan.units, plan.q2 * plan.q1, G), bf16),
-            pltpu.VMEM((plan.units, plan.q2 * plan.q1, G), bf16),
+            pltpu.VMEM((plan.groups, plan.seqs * plan.here, G), bf16),
+            pltpu.VMEM((plan.span, plan.seqs * plan.here, G), bf16),
+            pltpu.VMEM((plan.span, plan.seqs * plan.q2 * plan.q1, G), bf16),
+            pltpu.VMEM((plan.span, plan.seqs * plan.q2 * plan.q1, G), bf16),
             dma((4,)),
             dma((IN_CHUNKS,)),
-            dma((OUT_CHUNKS,)),
-            dma((plan.devices,)),
-            dma((plan.devices,)),
-            dma((plan.units,)),
-            dma((plan.units,)),
+            dma((1,)),
+            dma((plan.span,)),
+            dma((plan.span,)),
+            dma((plan.span,)),
+            dma((plan.span,)),
         ],
         compiler_params=pltpu.CompilerParams(
             collective_id=0, has_side_effects=True, vmem_limit_bytes=VMEM_BYTES

time: 19.1 us -> 17.6 us (0.921)
  Pallas kernels: 18.3 us -> 16.8 us
    pallas_call x1, Pallas kernels: 18.3 us -> 16.8 us  [kernel_body(): pl.pallas_call(functools.partial(mix_kernel, plan), out_shape=jax.ShapeDt...]
where the time goes in v3:
time: 17.6 us; the launch traced here: 17.4 us
  Pallas kernels  16.8 us (95%)
  local copies, waits for them, and re-layouts  0.66 us (4%)
    pallas_call x1, Pallas kernels, kernel_body(): pl.pallas_call(functools.partial(mix_kernel, plan), out_shape=jax.ShapeDt...  16.8 us
    unnamed x1, local copies, waits for them, and re-layouts  0.66 us

profile of v3, /device:TPU:0, one launch (start us, length us, event | category | flops | bytes accessed | tf_op | source)
XLA Modules:
  0.0 17.4 jit_solution(6955528227800174237)
XLA Ops:
  0.0 16.8 %shard_map.64 = bf16[2,2,8,2048]{3,2,1,0:T(8,128)(2,1)S(1)} custom-call(bf16[2,4,4,2048]{3,2,1,0:T(4,128)(2,1)} %tokens_hbm.1, bf16[2048]{0:T(1024)(128)(2,1)} %gain_hbm.1, bf16[2048,1024]{1,0:T(8,128)(2,1)} %w_in_hbm.1, bf16[1024,2048]{1,0:T(8,128)(2,1)} %w_out_hbm.1, bf16[2,2,512,256]{3,2,1,0:T(8,128)(2,1)} %constant.4.clone.table_hbm, ...), custom_call_target="tpu_custom_call" | custom-call | tf_op jit(solution)/shard_map/pallas_call | solution.py:331
  16.8 0.7 %copy.8 = bf16[2,2,8,2048]{3,2,1,0:T(8,128)(2,1)} copy(bf16[2,2,8,2048]{3,2,1,0:T(8,128)(2,1)S(1)} %shard_map.64) | data formatting | bytes 262144

commit v4 on v3

--- a/solution.py
+++ b/solution.py
@@ -263,8 +263,14 @@
             device_id_type=MESH,
         )
 
-    for mask in x_masks:
-        x_copy(me, partner(mask)).start()
+    for to_half in range(2):
+        for mask in [m for m in x_masks if m < plan.span]:
+            x_copy(me, to_half * plan.span + lax.rem(partner(mask), plan.span)).start()
+
+        @pl.when(half != to_half)
+        def _():
+            x_copy(me, to_half * plan.span + in_half).start()
+
     x_recv[in_side(me)] = x_send[group_of(me)]
     table_load.wait()
     channel_load.wait()
@@ -296,8 +302,12 @@
             device_id_type=MESH,
         )
 
-    for mask in s_masks:
-        s_copy(in_half, lax.rem(partner(mask), plan.span)).start()
+    for target in range(plan.span):
+
+        @pl.when(in_half != target)
+        def _(target=target):
+            s_copy(in_half, target).start()
+
     s_recv[in_half] = s_send[in_half]
     out_load.wait()
     for mask in reversed(s_masks):

time: 17.6 us -> 17.4 us (0.989)
  Pallas kernels: 16.8 us -> 16.6 us
where the time goes in v4:
time: 17.4 us; the launch traced here: 17.3 us
  Pallas kernels  16.6 us (95%)
  local copies, waits for them, and re-layouts  0.66 us (4%)
    pallas_call x1, Pallas kernels, kernel_body(): pl.pallas_call(functools.partial(mix_kernel, plan), out_shape=jax.ShapeDt...  16.6 us
    unnamed x1, local copies, waits for them, and re-layouts  0.66 us

profile of v4, /device:TPU:0, one launch (start us, length us, event | category | flops | bytes accessed | tf_op | source)
XLA Modules:
  0.0 17.3 jit_solution(2041935770132345711)
XLA Ops:
  0.0 16.6 %shard_map.64 = bf16[2,2,8,2048]{3,2,1,0:T(8,128)(2,1)S(1)} custom-call(bf16[2,4,4,2048]{3,2,1,0:T(4,128)(2,1)} %tokens_hbm.1, bf16[2048]{0:T(1024)(128)(2,1)} %gain_hbm.1, bf16[2048,1024]{1,0:T(8,128)(2,1)} %w_in_hbm.1, bf16[1024,2048]{1,0:T(8,128)(2,1)} %w_out_hbm.1, bf16[2,2,512,256]{3,2,1,0:T(8,128)(2,1)} %constant.4.clone.table_hbm, ...), custom_call_target="tpu_custom_call" | custom-call | tf_op jit(solution)/shard_map/pallas_call | solution.py:341
  16.6 0.7 %copy.8 = bf16[2,2,8,2048]{3,2,1,0:T(8,128)(2,1)} copy(bf16[2,2,8,2048]{3,2,1,0:T(8,128)(2,1)S(1)} %shard_map.64) | data formatting | bytes 262144
